TPU v7x, 32 devices: a whole 2x2x4 slice. The times are simulated.
32 devices in a mesh: ra: 8 (over z, x), cb: 4 (over y, core).
Axes of the slice: x: 2, y: 2, z: 4, core: 2. Of those that a mesh axis runs over, the one named last changes fastest.
Arguments:
- stream: bfloat16 [128, 2048], P(None, 'ra'), may hold values from -6 to 6
- gain_first: float32 [2048], P('ra'), may hold values from 0.5 to 1.5
- lift_first: bfloat16 [2048, 8192], P('ra', 'cb'), may hold values from -0.125 to 0.125
- drop_first: bfloat16 [8192, 2048], P('cb', 'ra'), may hold values from -0.0625 to 0.0625
- gain_second: float32 [2048], P('ra'), may hold values from 0.5 to 1.5
- lift_second: bfloat16 [2048, 8192], P('ra', 'cb'), may hold values from -0.125 to 0.125
- drop_second: bfloat16 [8192, 2048], P('cb', 'ra'), may hold values from -0.0625 to 0.0625
Outputs:
- stream_out: bfloat16 [128, 2048], P(None, 'ra')
All inputs are finite; a program needn't handle non-finite values.
Results may differ from a plain program's by a relative error of at most 0.0075.
Values may be sent and summed in bfloat16 or wider, within the bound.
A program may use at most 64 MiB of HBM per device.

v0:
```python
import jax
import jax.numpy as jnp
from jax import lax
from jax.sharding import PartitionSpec as P

residual_scale = 0.25
epsilon = 1e-06


def sublayer(stream, gain_vector, lift_weight, drop_weight):
    tile_count = lax.axis_size("ra")
    feature_count = stream.shape[1] * tile_count
    widened = stream.astype(jnp.float32)
    local_squares = jnp.sum(widened * widened, axis=1, keepdims=True)
    gained = (widened * gain_vector.astype(jnp.float32)).astype(jnp.bfloat16)
    total_squares = lax.psum(local_squares, "ra")
    extras = ()
    products = jnp.dot(gained, lift_weight, preferred_element_type=jnp.float32)
    summed = lax.psum((products,) + extras, "ra")
    pre_act = summed[0]
    pre_act = pre_act * lax.rsqrt(total_squares / feature_count + epsilon)
    hidden = jnp.square(jnp.maximum(pre_act, 0.0)).astype(jnp.bfloat16)
    branch_part = jnp.dot(hidden, drop_weight, preferred_element_type=jnp.float32)
    branch = lax.psum(branch_part, "cb")
    return (residual_scale * widened + branch).astype(jnp.bfloat16)


def on_device(stream, gain_first, lift_first, drop_first, gain_second, lift_second, drop_second):
    middle = sublayer(stream, gain_first, lift_first, drop_first)
    return sublayer(middle, gain_second, lift_second, drop_second)


def solution(mesh):
    return jax.shard_map(
        on_device,
        mesh=mesh,
        in_specs=(
            P(None, "ra"),
            P("ra"),
            P("ra", "cb"),
            P("cb", "ra"),
            P("ra"),
            P("ra", "cb"),
            P("cb", "ra"),
        ),
        out_specs=P(None, "ra"),
        check_vma=False,
    )
```

profile of v0, /device:TPU:0, one launch (start us, length us, event | category | flops | bytes accessed | tf_op | source)
XLA Modules:
  0.0 249.9 jit_solution(11339513205265086459)
XLA Ops:
  6.5 0.0 copy-start
  6.5 0.0 all-reduce.5.cloned.1.call-start
  6.5 1.2 copy-done
  7.8 0.0 copy-start.4
  7.8 2.3 fusion.16
  10.0 0.0 copy-start.1
  10.0 0.0 all-reduce.5.cloned.1.call-update
  10.0 0.0 all-reduce.7.cloned.1.call-start
  10.1 0.0 copy-done.4
  10.1 0.1 fusion.9
  10.2 23.6 %psum.43 = f32[128,1]{0,1:T(1,128)S(1)} all-reduce(f32[128,1]{0,1:T(1,128)S(1)} %bitcast.11), channel_id=1, replica_groups=mesh['ra'=8,'cb'=4] {'ra'}, use_global_device_ids=true, to_apply=%region_2.0 | all-reduce | flops 128 | bytes 1024 | tf_op jit(solution)/shard_map/psum | solution.py:16
  33.8 0.0 copy-start.3
  33.8 58.4 %all-reduce.5.cloned.1.call-done = f32[128,2048]{1,0:T(8,128)} async-done(((f32[128,2048]{1,0:T(8,128)}), f32[128,2048]{1,0:T(8,128)}) %all-reduce.5.cloned.1.call-update) | async-done | bytes 1048592 | tf_op jit(solution)/shard_map/psum | solution.py:19
  92.2 0.0 copy-done.1
  92.2 2.2 fusion
  94.4 0.0 all-reduce.7.cloned.1.call-update
  94.4 0.0 all-reduce.9.cloned.1.call-start
  94.5 31.5 %all-reduce.7.cloned.1.call-done = f32[128,256]{1,0:T(8,128)} async-done(((f32[128,256]{1,0:T(8,128)}), f32[128,256]{1,0:T(8,128)}) %all-reduce.7.cloned.1.call-update) | async-done | bytes 131088 | tf_op jit(solution)/shard_map/psum | solution.py:24
  126.0 1.0 fusion.13
  127.0 0.0 copy-start.5
  127.0 0.0 copy-done.3
  127.0 0.7 copy-done.5
  127.7 1.3 fusion.14
  129.0 0.0 all-reduce.9.cloned.1.call-update
  129.1 0.0 all-reduce.11.cloned.1.call-start
  129.1 21.7 %psum.46 = f32[128,1]{0,1:T(1,128)S(1)} all-reduce(f32[128,1]{0,1:T(1,128)S(1)} %bitcast.10), channel_id=1, replica_groups=mesh['ra'=8,'cb'=4] {'ra'}, use_global_device_ids=true, to_apply=%region_6.0 | all-reduce | flops 128 | bytes 1024 | tf_op jit(solution)/shard_map/psum | solution.py:16
  150.9 57.1 %all-reduce.9.cloned.1.call-done = f32[128,2048]{1,0:T(8,128)} async-done(((f32[128,2048]{1,0:T(8,128)}), f32[128,2048]{1,0:T(8,128)}) %all-reduce.9.cloned.1.call-update) | async-done | bytes 1048592 | tf_op jit(solution)/shard_map/psum | solution.py:19
  208.0 0.0 copy-done.2
  208.0 2.2 fusion.1
  210.2 0.0 all-reduce.11.cloned.1.call-update
  210.3 31.6 %all-reduce.11.cloned.1.call-done = f32[128,256]{1,0:T(8,128)} async-done(((f32[128,256]{1,0:T(8,128)}), f32[128,256]{1,0:T(8,128)}) %all-reduce.11.cloned.1.call-update) | async-done | bytes 131088 | tf_op jit(solution)/shard_map/psum | solution.py:24
  241.8 1.5 fusion.11
  (3 shorter events, 0.0 us)
Async XLA Ops:
  6.5 1.2 copy-start
  6.5 85.6 %all-reduce.5.cloned.1.call-start = ((), (), s32[]{:S(2)}) async-start(), calls=%async_computation | async-start | bytes 2097152 | tf_op jit(solution)/shard_map/psum | solution.py:19
  7.8 2.3 copy-start.4
  10.0 82.2 %copy-start.1 = (bf16[2048,256]{1,0:T(8,128)(2,1)S(1)}, bf16[2048,256]{1,0:T(8,128)(2,1)}, u32[]{:S(2)}) copy-start(bf16[2048,256]{1,0:T(8,128)(2,1)} %param.10) | copy-start | bytes 3145732
  10.0 115.9 %all-reduce.7.cloned.1.call-start = ((), (), s32[]{:S(2)}) async-start(), calls=%async_computation.1 | async-start | bytes 262144 | tf_op jit(solution)/shard_map/psum | solution.py:24
  33.8 93.2 %copy-start.3 = (bf16[256,2048]{1,0:T(8,128)(2,1)S(1)}, bf16[256,2048]{1,0:T(8,128)(2,1)}, u32[]{:S(2)}) copy-start(bf16[256,2048]{1,0:T(8,128)(2,1)} %param.12) | copy-start | bytes 3145732
  94.4 113.6 %all-reduce.9.cloned.1.call-start = ((), (), s32[]{:S(2)}) async-start(), calls=%async_computation.2 | async-start | bytes 2097152 | tf_op jit(solution)/shard_map/psum | solution.py:19
  127.0 0.7 copy-start.5
  129.0 79.0 %copy-start.2 = (bf16[2048,256]{1,0:T(8,128)(2,1)S(1)}, bf16[2048,256]{1,0:T(8,128)(2,1)}, u32[]{:S(2)}) copy-start(bf16[2048,256]{1,0:T(8,128)(2,1)} %param.13) | copy-start | bytes 3145732
  129.1 112.7 %all-reduce.11.cloned.1.call-start = ((), (), s32[]{:S(2)}) async-start(), calls=%async_computation.3 | async-start | bytes 262144 | tf_op jit(solution)/shard_map/psum | solution.py:24
Sparse Core Ops, SparseCore 0:
  10.8 81.2 all-reduce.4
  94.5 31.4 all-reduce.6
  129.5 78.4 all-reduce.8
  210.4 31.3 all-reduce.10
where the time goes:
time: 250 us
  waiting for transfers between devices  179 us (72%)
  blocking collectives  45.3 us (18%)
  between operations  13.2 us (5%)
  matrix products  8.05 us (3%)
  other arithmetic  2.68 us (1%)
    psum x2, waiting for transfers between devices, sublayer(): summed = lax.psum((products,) + extras, 'ra')  116 us
    psum x2, waiting for transfers between devices, sublayer(): branch = lax.psum(branch_part, 'cb')  63.1 us
    psum x2, blocking collectives, sublayer(): total_squares = lax.psum(local_squares, 'ra')  45.3 us
  transfers between devices with their start and end apart: 4, of which 4 were waited for; matrix products, arithmetic and copies ran while one was open for 0% of the time, Pallas kernels for 0%

commit v1 on v0

v1 whole, which is shorter than its diff:
```python
import functools

import jax
import jax.numpy as jnp
from jax import lax
from jax.experimental import pallas as pl
from jax.experimental.pallas import tpu as pltpu
from jax.sharding import PartitionSpec as P

residual_scale = 0.25
epsilon = 1e-06
MESH = pl.DeviceIdType.MESH
EXT = 128
GROUPS = 2
TILE = 512


def split_of(count):
    best = 1
    for d in range(1, count + 1):
        if count % d == 0 and d * d <= count:
            best = d
    return best


def widened_block(value):
    return value.astype(jnp.float32)


def kernel(cfg, stream_ref, gain0, gain1, lift0_h, drop0_h, lift1_h, drop1_h, out_ref,
           lift0, drop0, lift1, drop1, s_buf, xsend, xrecv, pown, sqown, zsend, zrecv, hid,
           csend, crecv, ybuf,
           wsem, xs_sem, xr_sem, zs_sem, zr_sem, hzs, hzr, hxs, hxr, cs_sem, cr_sem, ys_sem, yr_sem):
    nz, nx, ny, nc, G, Tg, Tt, H, D = cfg
    r = lax.axis_index("ra")
    c = lax.axis_index("cb")
    z, x = r // nx, lax.rem(r, nx)
    y, core = c // nc, lax.rem(c, nc)

    loads = []
    for i, (src, dst) in enumerate(((lift0_h, lift0), (drop0_h, drop0), (lift1_h, lift1), (drop1_h, drop1))):
        cp = pltpu.make_async_copy(src, dst, wsem.at[i])
        cp.start()
        loads.append(cp)

    zp = [lax.rem(z + k, nz) for k in range(nz)]
    zm = [lax.rem(z + nz - k, nz) for k in range(nz)]
    xp = [lax.rem(x + m, nx) for m in range(nx)]
    xm = [lax.rem(x + nx - m, nx) for m in range(nx)]
    zdev = [(zp[k] * nx + x, c) for k in range(nz)]
    xdev = [(z * nx + xp[m], c) for m in range(nx)]
    cdev = (r, y * nc + lax.rem(core + 1, nc))
    ydev = [(r, lax.rem(y + j, ny) * nc + core) for j in range(ny)]
    peers = [zdev[k] for k in range(1, nz)] + [xdev[m] for m in range(1, nx)] + [cdev] + [ydev[j] for j in range(1, ny)]
    order = sorted(range(1, nz), key=lambda k: (abs(k - nz // 2), k))

    barrier = pltpu.get_barrier_semaphore()
    for dev in peers:
        pl.semaphore_signal(barrier, inc=1, device_id=dev, device_id_type=MESH)

    gains = (gain0, gain1)
    lifts = (lift0, lift1)
    drops = (drop0, drop1)
    half = nz * Tt
    pending = []

    def remote(src, dst, ssem, rsem, dev):
        cp = pltpu.make_async_remote_copy(src_ref=src, dst_ref=dst, send_sem=ssem, recv_sem=rsem,
                                          device_id=dev, device_id_type=MESH)
        cp.start()
        pending.append(cp)
        return cp

    lane = lax.broadcasted_iota(jnp.int32, (1, EXT), 1)

    def pack_sq(sq):
        hi = sq.astype(jnp.bfloat16).astype(jnp.float32)
        return jnp.where(lane < EXT // 2, hi, sq - hi).astype(jnp.bfloat16)

    def unpack_sq(ext):
        e = ext.astype(jnp.float32)
        return e[:, 0:1] + e[:, EXT // 2:EXT // 2 + 1]

    xcp, zcp, hzc, hxc, ccp, ycp = {}, {}, {}, {}, {}, {}

    def s1(l, g):
        gain = gains[l][...]
        w = lifts[l]
        for m in [*range(1, nx), 0]:
            rows = pl.ds(pl.multiple_of(xp[m] * half, half), half)
            s = s_buf[l, g, rows, :]
            sq = jnp.sum(s * s, axis=1, keepdims=True)
            gd = (s * gain).astype(jnp.bfloat16)
            if m == 0:
                for zz in range(nz):
                    sqown[l, g, zz] = jnp.broadcast_to(sq[zz * Tt:(zz + 1) * Tt], (Tt, EXT))
            else:
                ext = pack_sq(sq)
                for zz in range(nz):
                    xsend[l, g, m - 1, zz, :, H:] = ext[zz * Tt:(zz + 1) * Tt]
            for t in range(0, H, TILE):
                p = jnp.dot(gd, w[:, t:t + TILE], preferred_element_type=jnp.float32)
                for zz in range(nz):
                    part = p[zz * Tt:(zz + 1) * Tt]
                    if m == 0:
                        pown[l, g, zz, :, t:t + TILE] = part
                    else:
                        xsend[l, g, m - 1, zz, :, t:t + TILE] = part.astype(jnp.bfloat16)
            if m > 0:
                for k in order + [0]:
                    xcp[l, g, m, k] = remote(xsend.at[l, g, m - 1, zp[k]], xrecv.at[l, g, m - 1, zp[k]],
                                             xs_sem.at[l, g, m - 1, k], xr_sem.at[l, g, m - 1, k], xdev[m])

    def xsum(l, g, k):
        for m in range(1, nx):
            xcp[l, g, m, k].wait_recv()
        acc = pown[l, g, zp[k]]
        sq = sqown[l, g, zp[k]][:, 0:1]
        for m in range(1, nx):
            acc = acc + xrecv[l, g, m - 1, zp[k], :, :H].astype(jnp.float32)
            sq = sq + unpack_sq(xrecv[l, g, m - 1, zp[k], :, H:])
        return acc, sq

    def s2(l, g):
        for k in order:
            acc, sq = xsum(l, g, k)
            zsend[l, g, k - 1, :, :H] = acc.astype(jnp.bfloat16)
            zsend[l, g, k - 1, :, H:] = pack_sq(sq)
            zcp[l, g, k] = remote(zsend.at[l, g, k - 1], zrecv.at[l, g, k - 1],
                                  zs_sem.at[l, g, k - 1], zr_sem.at[l, g, k - 1], zdev[k])

    def s3(l, g):
        acc, sq = xsum(l, g, 0)
        for k in order:
            zcp[l, g, k].wait_recv()
            acc = acc + zrecv[l, g, k - 1, :, :H].astype(jnp.float32)
            sq = sq + unpack_sq(zrecv[l, g, k - 1, :, H:])
        pre = acc * lax.rsqrt(sq / D + epsilon)
        b = x * nz + z
        hid[l, g, b] = jnp.square(jnp.maximum(pre, 0.0)).astype(jnp.bfloat16)
        for k in order:
            hzc[l, g, k] = remote(hid.at[l, g, b], hid.at[l, g, b], hzs.at[l, g, k - 1], hzr.at[l, g, k - 1], zdev[k])
        for m in range(1, nx):
            hxc[l, g, m, 0] = remote(hid.at[l, g, b], hid.at[l, g, b], hxs.at[l, g, m - 1, 0], hxr.at[l, g, m - 1, 0], xdev[m])

    def s4(l, g):
        for k in order:
            hzc[l, g, k].wait_recv()
            b = x * nz + zm[k]
            for m in range(1, nx):
                hxc[l, g, m, k] = remote(hid.at[l, g, b], hid.at[l, g, b], hxs.at[l, g, m - 1, k], hxr.at[l, g, m - 1, k], xdev[m])

    def s5(l, g):
        for m in range(1, nx):
            for k in [0] + order:
                hxc[l, g, m, k].wait_recv()
        h = hid[l, g]
        if Tt % 16 == 0:
            h = h.reshape(Tg, H)
        else:
            h = h.astype(jnp.float32).reshape(Tg, H).astype(jnp.bfloat16)
        csend[l, g] = jnp.dot(h, drops[l][...], preferred_element_type=jnp.float32)
        ccp[l, g] = remote(csend.at[l, g], crecv.at[l, g], cs_sem.at[l, g], cr_sem.at[l, g], cdev)

    def s6(l, g):
        ccp[l, g].wait_recv()
        ybuf[l, g, y] = (csend[l, g] + crecv[l, g]).astype(jnp.bfloat16)
        for j in range(1, ny):
            ycp[l, g, j] = remote(ybuf.at[l, g, y], ybuf.at[l, g, y], ys_sem.at[l, g, j - 1], yr_sem.at[l, g, j - 1], ydev[j])

    def s7(l, g):
        for j in range(1, ny):
            ycp[l, g, j].wait_recv()
        total = ybuf[l, g, 0].astype(jnp.float32)
        for j in range(1, ny):
            total = total + ybuf[l, g, j].astype(jnp.float32)
        res = (residual_scale * s_buf[l, g] + total).astype(jnp.bfloat16)
        if l == 0:
            s_buf[1, g] = res.astype(jnp.float32)
        else:
            out_ref[g * Tg:(g + 1) * Tg, :] = res

    for g in range(G):
        s_buf[0, g] = stream_ref[g * Tg:(g + 1) * Tg, :].astype(jnp.float32)
    pl.semaphore_wait(barrier, len(peers))
    loads[0].wait()
    for g in range(G):
        s1(0, g)
    for l in range(2):
        for stage in (s2, s3, s4):
            for g in range(G):
                stage(l, g)
        if l == 0:
            for i in range(1, 4):
                loads[i].wait()
        for stage in (s5, s6):
            for g in range(G):
                stage(l, g)
        for g in range(G):
            s7(l, g)
            if l == 0:
                s1(1, g)
    for cp in pending:
        cp.wait_send()


def on_device(nra, ncb, stream, gain_first, lift_first, drop_first, gain_second, lift_second, drop_second):
    nx = split_of(nra)
    nz = nra // nx
    nc = 2
    ny = ncb // nc
    T, Dl = stream.shape
    H = lift_first.shape[1]
    G = GROUPS if T % (GROUPS * nra * 8) == 0 else 1
    Tg = T // G
    Tt = Tg // nra
    L = 2
    cfg = (nz, nx, ny, nc, G, Tg, Tt, H, Dl * nra)
    bf, f32 = jnp.bfloat16, jnp.float32
    dma = pltpu.SemaphoreType.DMA
    vm = pl.BlockSpec(memory_space=pltpu.VMEM)
    hbm = pl.BlockSpec(memory_space=pl.ANY)
    wide = H + EXT
    scratch = [
        pltpu.VMEM(lift_first.shape, bf), pltpu.VMEM(drop_first.shape, bf),
        pltpu.VMEM(lift_second.shape, bf), pltpu.VMEM(drop_second.shape, bf),
        pltpu.VMEM((L, G, Tg, Dl), f32),
        pltpu.VMEM((L, G, nx - 1, nz, Tt, wide), bf),
        pltpu.VMEM((L, G, nx - 1, nz, Tt, wide), bf),
        pltpu.VMEM((L, G, nz, Tt, H), f32),
        pltpu.VMEM((L, G, nz, Tt, EXT), f32),
        pltpu.VMEM((L, G, nz - 1, Tt, wide), bf),
        pltpu.VMEM((L, G, nz - 1, Tt, wide), bf),
        pltpu.VMEM((L, G, nra, Tt, H), bf),
        pltpu.VMEM((L, G, Tg, Dl), f32),
        pltpu.VMEM((L, G, Tg, Dl), f32),
        pltpu.VMEM((L, G, ny, Tg, Dl), bf),
        dma((4,)),
        dma((L, G, nx - 1, nz)), dma((L, G, nx - 1, nz)),
        dma((L, G, nz - 1)), dma((L, G, nz - 1)),
        dma((L, G, nz - 1)), dma((L, G, nz - 1)),
        dma((L, G, nx - 1, nz)), dma((L, G, nx - 1, nz)),
        dma((L, G)), dma((L, G)),
        dma((L, G, ny - 1)), dma((L, G, ny - 1)),
    ]
    return pl.pallas_call(
        functools.partial(kernel, cfg),
        out_shape=jax.ShapeDtypeStruct((T, Dl), bf),
        in_specs=[vm, vm, vm, hbm, hbm, hbm, hbm],
        out_specs=vm,
        scratch_shapes=scratch,
        compiler_params=pltpu.CompilerParams(collective_id=0, has_side_effects=True,
                                             vmem_limit_bytes=48 * 1024 * 1024),
    )(stream, gain_first.reshape(1, -1), gain_second.reshape(1, -1), lift_first, drop_first, lift_second, drop_second)


def solution(mesh):
    return jax.shard_map(
        functools.partial(on_device, mesh.shape["ra"], mesh.shape["cb"]),
        mesh=mesh,
        in_specs=(
            P(None, "ra"),
            P("ra"),
            P("ra", "cb"),
            P("cb", "ra"),
            P("ra"),
            P("ra", "cb"),
            P("cb", "ra"),
        ),
        out_specs=P(None, "ra"),
        check_vma=False,
    )
```

time: 250 us -> 62.1 us (0.25)
  waiting for transfers between devices: 179 us -> 0 us
  Pallas kernels: 0 us -> 54.7 us
  blocking collectives: 45.3 us -> 0 us
  between operations: 13.2 us -> 0.02 us
  matrix products: 8.05 us -> 0 us
  local copies, waits for them, and re-layouts: 1.91 us -> 7.06 us
  other arithmetic: 2.68 us -> 0 us
    psum x4 -> x0, waiting for transfers between devices: 179 us -> none  [the longest x2 116 us: sublayer(): summed = lax.psum((products,) + extras, 'ra')]
    pallas_call x0 -> x1, Pallas kernels: none -> 54.7 us  [on_device(): pl.pallas_call(functools.partial(kernel, cfg), out_shape=jax.ShapeDtypeSt...]
    psum x2 -> x0, blocking collectives: 45.3 us -> none  [sublayer(): total_squares = lax.psum(local_squares, 'ra')]
    dot_general x4 -> x0, matrix products: 8.05 us -> none  [the longest x2 4.45 us: sublayer(): jnp.dot(hidden, drop_weight, preferred_element_type=jnp.float32)]
    unnamed x12 -> x15, local copies, waits for them, and re-layouts: 1.91 us -> 7.06 us
  transfers between devices with their start and end apart: 4 -> 0, of which waited for: 4 -> 0; matrix products, arithmetic and copies ran while one was open for 0% -> 0% of each run, Pallas kernels for 0% -> 0%
where the time goes in v1:
time: 62.1 us; the launch traced here: 61.8 us
  Pallas kernels  54.7 us (88%)
  local copies, waits for them, and re-layouts  7.06 us (11%)
    pallas_call x1, Pallas kernels, on_device(): pl.pallas_call(functools.partial(kernel, cfg), out_shape=jax.ShapeDtypeSt...  54.7 us
    unnamed x15, local copies, waits for them, and re-layouts  7.06 us

profile of v1, /device:TPU:0, one launch (start us, length us, event | category | flops | bytes accessed | tf_op | source)
XLA Modules:
  0.0 61.8 jit_solution(15479410573023626454)
XLA Ops:
  0.0 0.0 copy-start.6
  0.0 0.0 copy-start.5
  0.0 0.7 %copy-done.6 = f32[256]{0:T(256)S(1)} copy-done((f32[256]{0:T(256)S(1)}, f32[256]{0:T(256)}, u32[]{:S(2)}) %copy-start.6) | copy-done | bytes 1048
  0.7 0.0 copy-done.5
  0.7 0.0 copy-start
  0.7 1.2 %copy-done = bf16[256,2048]{1,0:T(8,128)(2,1)S(1)} copy-done((bf16[256,2048]{1,0:T(8,128)(2,1)S(1)}, bf16[256,2048]{1,0:T(8,128)(2,1)}, u32[]{:S(2)}) %copy-start) | copy-done | bytes 1048600
  1.9 0.0 copy-start.1
  1.9 1.2 %copy-done.1 = bf16[2048,256]{1,0:T(8,128)(2,1)S(1)} copy-done((bf16[2048,256]{1,0:T(8,128)(2,1)S(1)}, bf16[2048,256]{1,0:T(8,128)(2,1)}, u32[]{:S(2)}) %copy-start.1) | copy-done | bytes 1048600
  3.1 0.0 copy-start.2
  3.1 1.2 %copy-done.2 = bf16[256,2048]{1,0:T(8,128)(2,1)S(1)} copy-done((bf16[256,2048]{1,0:T(8,128)(2,1)S(1)}, bf16[256,2048]{1,0:T(8,128)(2,1)}, u32[]{:S(2)}) %copy-start.2) | copy-done | bytes 1048600
  4.4 0.0 copy-start.3
  4.4 1.2 %copy-done.3 = bf16[2048,256]{1,0:T(8,128)(2,1)S(1)} copy-done((bf16[2048,256]{1,0:T(8,128)(2,1)S(1)}, bf16[2048,256]{1,0:T(8,128)(2,1)}, u32[]{:S(2)}) %copy-start.3) | copy-done | bytes 1048600
  5.6 0.0 copy-start.4
  5.6 0.8 %copy-done.4 = bf16[128,256]{1,0:T(8,128)(2,1)S(1)} copy-done((bf16[128,256]{1,0:T(8,128)(2,1)S(1)}, bf16[128,256]{1,0:T(8,128)(2,1)}, u32[]{:S(2)}) %copy-start.4) | copy-done | bytes 65560
  6.4 54.7 %shard_map.73 = bf16[128,256]{1,0:T(8,128)(2,1)S(1)} custom-call(bf16[128,256]{1,0:T(8,128)(2,1)S(1)} %copy-done.4, f32[1,256]{1,0:T(1,128)S(1)} %bitcast.2, f32[1,256]{1,0:T(1,128)S(1)} %bitcast.3, bf16[256,2048]{1,0:T(8,128)(2,1)S(1)} %copy-done, bf16[2048,256]{1,0:T(8,128)(2,1)S(1)} %copy-done.1, bf16[256,2048]{1,0:T(8,128)(2,1)S(1)} %copy-done.2, ...), custom_call_target="tpu_custom_call" | custom-call | tf_op jit(solution)/shard_map/pallas_call | solution.py:246
  61.1 0.6 %copy.9 = bf16[128,256]{1,0:T(8,128)(2,1)} copy(bf16[128,256]{1,0:T(8,128)(2,1)S(1)} %shard_map.73) | data formatting | bytes 131072
Async XLA Ops:
  0.0 0.7 %copy-start.6 = (f32[256]{0:T(256)S(1)}, f32[256]{0:T(256)}, u32[]{:S(2)}) copy-start(f32[256]{0:T(256)} %param.11) | copy-start | bytes 3076
  0.0 0.7 %copy-start.5 = (f32[256]{0:T(256)S(1)}, f32[256]{0:T(256)}, u32[]{:S(2)}) copy-start(f32[256]{0:T(256)} %param.8) | copy-start | bytes 3076
  0.7 1.2 %copy-start = (bf16[256,2048]{1,0:T(8,128)(2,1)S(1)}, bf16[256,2048]{1,0:T(8,128)(2,1)}, u32[]{:S(2)}) copy-start(bf16[256,2048]{1,0:T(8,128)(2,1)} %lift0_h.1) | copy-start | bytes 3145732
  1.9 1.2 %copy-start.1 = (bf16[2048,256]{1,0:T(8,128)(2,1)S(1)}, bf16[2048,256]{1,0:T(8,128)(2,1)}, u32[]{:S(2)}) copy-start(bf16[2048,256]{1,0:T(8,128)(2,1)} %drop0_h.1) | copy-start | bytes 3145732
  3.1 1.2 %copy-start.2 = (bf16[256,2048]{1,0:T(8,128)(2,1)S(1)}, bf16[256,2048]{1,0:T(8,128)(2,1)}, u32[]{:S(2)}) copy-start(bf16[256,2048]{1,0:T(8,128)(2,1)} %lift1_h.1) | copy-start | bytes 3145732
  4.4 1.2 %copy-start.3 = (bf16[2048,256]{1,0:T(8,128)(2,1)S(1)}, bf16[2048,256]{1,0:T(8,128)(2,1)}, u32[]{:S(2)}) copy-start(bf16[2048,256]{1,0:T(8,128)(2,1)} %drop1_h.1) | copy-start | bytes 3145732
  5.6 0.8 %copy-start.4 = (bf16[128,256]{1,0:T(8,128)(2,1)S(1)}, bf16[128,256]{1,0:T(8,128)(2,1)}, u32[]{:S(2)}) copy-start(bf16[128,256]{1,0:T(8,128)(2,1)} %stream_ref.1) | copy-start | bytes 196612

commit v2 on v1

--- a/solution.py
+++ b/solution.py
@@ -13,6 +13,7 @@
 EXT = 128
 GROUPS = 2
 TILE = 512
+GRANT = 60 * 1024 * 1024
 
 
 def split_of(count):
@@ -23,12 +24,8 @@
     return best
 
 
-def widened_block(value):
-    return value.astype(jnp.float32)
-
-
-def kernel(cfg, stream_ref, gain0, gain1, lift0_h, drop0_h, lift1_h, drop1_h, out_ref,
-           lift0, drop0, lift1, drop1, s_buf, xsend, xrecv, pown, sqown, zsend, zrecv, hid,
+def kernel(cfg, stream_h, gain0_h, gain1_h, lift0_h, drop0_h, lift1_h, drop1_h, out_ref,
+           stream_ref, gain0, gain1, lift0, drop0, lift1, drop1, s_buf, xsend, xrecv, pown, sqown, zsend, zrecv, hid,
            csend, crecv, ybuf,
            wsem, xs_sem, xr_sem, zs_sem, zr_sem, hzs, hzr, hxs, hxr, cs_sem, cr_sem, ys_sem, yr_sem):
     nz, nx, ny, nc, G, Tg, Tt, H, D = cfg
@@ -38,7 +35,8 @@
     y, core = c // nc, lax.rem(c, nc)
 
     loads = []
-    for i, (src, dst) in enumerate(((lift0_h, lift0), (drop0_h, drop0), (lift1_h, lift1), (drop1_h, drop1))):
+    for i, (src, dst) in enumerate(((stream_h, stream_ref), (gain0_h, gain0), (lift0_h, lift0), (drop0_h, drop0),
+                                (gain1_h, gain1), (lift1_h, lift1), (drop1_h, drop1))):
         cp = pltpu.make_async_copy(src, dst, wsem.at[i])
         cp.start()
         loads.append(cp)
@@ -180,10 +178,12 @@
         else:
             out_ref[g * Tg:(g + 1) * Tg, :] = res
 
+    loads[0].wait()
     for g in range(G):
         s_buf[0, g] = stream_ref[g * Tg:(g + 1) * Tg, :].astype(jnp.float32)
+    loads[1].wait()
+    loads[2].wait()
     pl.semaphore_wait(barrier, len(peers))
-    loads[0].wait()
     for g in range(G):
         s1(0, g)
     for l in range(2):
@@ -191,7 +191,7 @@
             for g in range(G):
                 stage(l, g)
         if l == 0:
-            for i in range(1, 4):
+            for i in range(3, 7):
                 loads[i].wait()
         for stage in (s5, s6):
             for g in range(G):
@@ -222,6 +222,7 @@
     hbm = pl.BlockSpec(memory_space=pl.ANY)
     wide = H + EXT
     scratch = [
+        pltpu.VMEM((T, Dl), bf), pltpu.VMEM((1, Dl), f32), pltpu.VMEM((1, Dl), f32),
         pltpu.VMEM(lift_first.shape, bf), pltpu.VMEM(drop_first.shape, bf),
         pltpu.VMEM(lift_second.shape, bf), pltpu.VMEM(drop_second.shape, bf),
         pltpu.VMEM((L, G, Tg, Dl), f32),
@@ -235,7 +236,7 @@
         pltpu.VMEM((L, G, Tg, Dl), f32),
         pltpu.VMEM((L, G, Tg, Dl), f32),
         pltpu.VMEM((L, G, ny, Tg, Dl), bf),
-        dma((4,)),
+        dma((7,)),
         dma((L, G, nx - 1, nz)), dma((L, G, nx - 1, nz)),
         dma((L, G, nz - 1)), dma((L, G, nz - 1)),
         dma((L, G, nz - 1)), dma((L, G, nz - 1)),
@@ -246,11 +247,11 @@
     return pl.pallas_call(
         functools.partial(kernel, cfg),
         out_shape=jax.ShapeDtypeStruct((T, Dl), bf),
-        in_specs=[vm, vm, vm, hbm, hbm, hbm, hbm],
+        in_specs=[hbm] * 7,
         out_specs=vm,
         scratch_shapes=scratch,
         compiler_params=pltpu.CompilerParams(collective_id=0, has_side_effects=True,
-                                             vmem_limit_bytes=48 * 1024 * 1024),
+                                             vmem_limit_bytes=GRANT),
     )(stream, gain_first.reshape(1, -1), gain_second.reshape(1, -1), lift_first, drop_first, lift_second, drop_second)
 
 

time: 62.1 us -> 56.6 us (0.911)
  local copies, waits for them, and re-layouts: 7.06 us -> 1.47 us
    unnamed x15 -> x1, local copies, waits for them, and re-layouts: 7.06 us -> 1.47 us
where the time goes in v2:
time: 56.6 us; the launch traced here: 56.5 us
  Pallas kernels  55 us (97%)
  local copies, waits for them, and re-layouts  1.47 us (3%)
    pallas_call x1, Pallas kernels, on_device(): pl.pallas_call(functools.partial(kernel, cfg), out_shape=jax.ShapeDtypeSt...  55 us
    unnamed x1, local copies, waits for them, and re-layouts  1.47 us

profile of v2, /device:TPU:0, one launch (start us, length us, event | category | flops | bytes accessed | tf_op | source)
XLA Modules:
  0.0 56.5 jit_solution(6355706447162443988)
XLA Ops:
  0.0 55.0 %shard_map.73 = bf16[128,256]{1,0:T(8,128)(2,1)} custom-call(bf16[128,256]{1,0:T(8,128)(2,1)} %stream_h.1, f32[1,256]{1,0:T(1,128)} %bitcast.2, f32[1,256]{1,0:T(1,128)} %bitcast.3, bf16[256,2048]{1,0:T(8,128)(2,1)} %lift0_h.1, bf16[2048,256]{1,0:T(8,128)(2,1)} %drop0_h.1, bf16[256,2048]{1,0:T(8,128)(2,1)} %lift1_h.1, bf16[2048,256]{1,0:T(8,128)(2,1)} %drop1_h.1), custom_call_target="tpu_custom_call" | custom-call | tf_op jit(solution)/shard_map/pallas_call | solution.py:247
  55.0 1.5 %copy.9 = bf16[128,256]{1,0:T(8,128)(2,1)} copy(bf16[128,256]{1,0:T(8,128)(2,1)} %shard_map.73) | data formatting | bytes 131072

commit v3 on v2

--- a/solution.py
+++ b/solution.py
@@ -26,13 +26,12 @@
 
 def kernel(cfg, stream_h, gain0_h, gain1_h, lift0_h, drop0_h, lift1_h, drop1_h, out_ref,
            stream_ref, gain0, gain1, lift0, drop0, lift1, drop1, s_buf, xsend, xrecv, pown, sqown, zsend, zrecv, hid,
-           csend, crecv, ybuf,
-           wsem, xs_sem, xr_sem, zs_sem, zr_sem, hzs, hzr, hxs, hxr, cs_sem, cr_sem, ys_sem, yr_sem):
-    nz, nx, ny, nc, G, Tg, Tt, H, D = cfg
+           ybuf,
+           wsem, xs_sem, xr_sem, zs_sem, zr_sem, hzs, hzr, hxs, hxr, ys_sem, yr_sem):
+    nz, nx, ny, G, Tg, Tt, H, D = cfg
     r = lax.axis_index("ra")
     c = lax.axis_index("cb")
     z, x = r // nx, lax.rem(r, nx)
-    y, core = c // nc, lax.rem(c, nc)
 
     loads = []
     for i, (src, dst) in enumerate(((stream_h, stream_ref), (gain0_h, gain0), (lift0_h, lift0), (drop0_h, drop0),
@@ -47,9 +46,8 @@
     xm = [lax.rem(x + nx - m, nx) for m in range(nx)]
     zdev = [(zp[k] * nx + x, c) for k in range(nz)]
     xdev = [(z * nx + xp[m], c) for m in range(nx)]
-    cdev = (r, y * nc + lax.rem(core + 1, nc))
-    ydev = [(r, lax.rem(y + j, ny) * nc + core) for j in range(ny)]
-    peers = [zdev[k] for k in range(1, nz)] + [xdev[m] for m in range(1, nx)] + [cdev] + [ydev[j] for j in range(1, ny)]
+    ydev = [(r, lax.rem(c + j, ny)) for j in range(ny)]
+    peers = [zdev[k] for k in range(1, nz)] + [xdev[m] for m in range(1, nx)] + [ydev[j] for j in range(1, ny)]
     order = sorted(range(1, nz), key=lambda k: (abs(k - nz // 2), k))
 
     barrier = pltpu.get_barrier_semaphore()
@@ -79,7 +77,7 @@
         e = ext.astype(jnp.float32)
         return e[:, 0:1] + e[:, EXT // 2:EXT // 2 + 1]
 
-    xcp, zcp, hzc, hxc, ccp, ycp = {}, {}, {}, {}, {}, {}
+    xcp, zcp, hzc, hxc, ycp = {}, {}, {}, {}, {}
 
     def s1(l, g):
         gain = gains[l][...]
@@ -105,6 +103,8 @@
                     else:
                         xsend[l, g, m - 1, zz, :, t:t + TILE] = part.astype(jnp.bfloat16)
             if m > 0:
+                if l == 0 and g == 0 and m == 1:
+                    pl.semaphore_wait(barrier, len(peers))
                 for k in order + [0]:
                     xcp[l, g, m, k] = remote(xsend.at[l, g, m - 1, zp[k]], xrecv.at[l, g, m - 1, zp[k]],
                                              xs_sem.at[l, g, m - 1, k], xr_sem.at[l, g, m - 1, k], xdev[m])
@@ -157,14 +157,9 @@
             h = h.reshape(Tg, H)
         else:
             h = h.astype(jnp.float32).reshape(Tg, H).astype(jnp.bfloat16)
-        csend[l, g] = jnp.dot(h, drops[l][...], preferred_element_type=jnp.float32)
-        ccp[l, g] = remote(csend.at[l, g], crecv.at[l, g], cs_sem.at[l, g], cr_sem.at[l, g], cdev)
-
-    def s6(l, g):
-        ccp[l, g].wait_recv()
-        ybuf[l, g, y] = (csend[l, g] + crecv[l, g]).astype(jnp.bfloat16)
+        ybuf[l, g, c] = jnp.dot(h, drops[l][...], preferred_element_type=jnp.float32).astype(jnp.bfloat16)
         for j in range(1, ny):
-            ycp[l, g, j] = remote(ybuf.at[l, g, y], ybuf.at[l, g, y], ys_sem.at[l, g, j - 1], yr_sem.at[l, g, j - 1], ydev[j])
+            ycp[l, g, j] = remote(ybuf.at[l, g, c], ybuf.at[l, g, c], ys_sem.at[l, g, j - 1], yr_sem.at[l, g, j - 1], ydev[j])
 
     def s7(l, g):
         for j in range(1, ny):
@@ -183,7 +178,6 @@
         s_buf[0, g] = stream_ref[g * Tg:(g + 1) * Tg, :].astype(jnp.float32)
     loads[1].wait()
     loads[2].wait()
-    pl.semaphore_wait(barrier, len(peers))
     for g in range(G):
         s1(0, g)
     for l in range(2):
@@ -193,7 +187,7 @@
         if l == 0:
             for i in range(3, 7):
                 loads[i].wait()
-        for stage in (s5, s6):
+        for stage in (s5,):
             for g in range(G):
                 stage(l, g)
         for g in range(G):
@@ -207,15 +201,14 @@
 def on_device(nra, ncb, stream, gain_first, lift_first, drop_first, gain_second, lift_second, drop_second):
     nx = split_of(nra)
     nz = nra // nx
-    nc = 2
-    ny = ncb // nc
+    ny = ncb
     T, Dl = stream.shape
     H = lift_first.shape[1]
     G = GROUPS if T % (GROUPS * nra * 8) == 0 else 1
     Tg = T // G
     Tt = Tg // nra
     L = 2
-    cfg = (nz, nx, ny, nc, G, Tg, Tt, H, Dl * nra)
+    cfg = (nz, nx, ny, G, Tg, Tt, H, Dl * nra)
     bf, f32 = jnp.bfloat16, jnp.float32
     dma = pltpu.SemaphoreType.DMA
     vm = pl.BlockSpec(memory_space=pltpu.VMEM)
@@ -233,15 +226,12 @@
         pltpu.VMEM((L, G, nz - 1, Tt, wide), bf),
         pltpu.VMEM((L, G, nz - 1, Tt, wide), bf),
         pltpu.VMEM((L, G, nra, Tt, H), bf),
-        pltpu.VMEM((L, G, Tg, Dl), f32),
-        pltpu.VMEM((L, G, Tg, Dl), f32),
         pltpu.VMEM((L, G, ny, Tg, Dl), bf),
         dma((7,)),
         dma((L, G, nx - 1, nz)), dma((L, G, nx - 1, nz)),
         dma((L, G, nz - 1)), dma((L, G, nz - 1)),
         dma((L, G, nz - 1)), dma((L, G, nz - 1)),
         dma((L, G, nx - 1, nz)), dma((L, G, nx - 1, nz)),
-        dma((L, G)), dma((L, G)),
         dma((L, G, ny - 1)), dma((L, G, ny - 1)),
     ]
     return pl.pallas_call(

time: 56.6 us -> 53.7 us (0.949)
  Pallas kernels: 55 us -> 52.1 us
    pallas_call x1, Pallas kernels: 55 us -> 52.1 us  [on_device(): pl.pallas_call(functools.partial(kernel, cfg), out_shape=jax.ShapeDtypeSt...]
where the time goes in v3:
time: 53.7 us; the launch traced here: 53.6 us
  Pallas kernels  52.1 us (97%)
  local copies, waits for them, and re-layouts  1.47 us (3%)
    pallas_call x1, Pallas kernels, on_device(): pl.pallas_call(functools.partial(kernel, cfg), out_shape=jax.ShapeDtypeSt...  52.1 us
    unnamed x1, local copies, waits for them, and re-layouts  1.47 us

profile of v3, /device:TPU:0, one launch (start us, length us, event | category | flops | bytes accessed | tf_op | source)
XLA Modules:
  0.0 53.6 jit_solution(4757491753963793711)
XLA Ops:
  0.0 52.1 %shard_map.73 = bf16[128,256]{1,0:T(8,128)(2,1)} custom-call(bf16[128,256]{1,0:T(8,128)(2,1)} %stream_h.1, f32[1,256]{1,0:T(1,128)} %bitcast.2, f32[1,256]{1,0:T(1,128)} %bitcast.3, bf16[256,2048]{1,0:T(8,128)(2,1)} %lift0_h.1, bf16[2048,256]{1,0:T(8,128)(2,1)} %drop0_h.1, bf16[256,2048]{1,0:T(8,128)(2,1)} %lift1_h.1, bf16[2048,256]{1,0:T(8,128)(2,1)} %drop1_h.1), custom_call_target="tpu_custom_call" | custom-call | tf_op jit(solution)/shard_map/pallas_call | solution.py:237
  52.1 1.5 %copy.9 = bf16[128,256]{1,0:T(8,128)(2,1)} copy(bf16[128,256]{1,0:T(8,128)(2,1)} %shard_map.73) | data formatting | bytes 131072
